TPU v7x, 512 devices: a whole 4x4x16 slice. The times are simulated.
512 devices in a mesh: sp: 32 (over z, core), tp: 16 (over y, x).
Axes of the slice: x: 4, y: 4, z: 16, core: 2. Of those that a mesh axis runs over, the one named last changes fastest.
Arguments:
- layer_input: bfloat16 [32768, 4096], P('sp', 'tp'), may hold values from -6 to 6
- key_weight: bfloat16 [4096, 4096], P(None, 'tp'), may hold values from -0.09375 to 0.09375
- value_weight: bfloat16 [4096, 4096], P(None, 'tp'), may hold values from -0.09375 to 0.09375
- decay_exponent: float32 [32], P('tp'), may hold values from -0.077 to -4.2114258e-05, as said below
- query_new: bfloat16 [2, 4096], P(None, 'tp'), may hold values from -6 to 6
- key_new: bfloat16 [2, 4096], P(None, 'tp'), may hold values from -6 to 6
- value_new: bfloat16 [2, 4096], P(None, 'tp'), may hold values from -6 to 6
- norm_gain: float32 [4096], P('tp'), may hold values from 0.1 to 1.9
Outputs:
- state_cache: bfloat16 [2, 32, 128, 128], P(None, 'tp', 'sp')
- first_read: bfloat16 [2, 4096], P(None, 'tp')
Inputs may be any that keep to these rules, and one draw needn't show every extreme that they name: decay_exponent is negative.
All inputs are finite; a program needn't handle non-finite values.
Results may differ from a plain program's by a relative error of at most 0.011.
Values may be sent and summed in bfloat16 or wider, within the bound.
A program may use at most 64 MiB of HBM per device.

v0:
```python
import jax
import jax.numpy as jnp
from jax import lax
from jax.sharding import PartitionSpec as P

SEQS = 2


def in_blocks(x, dim, peers):
    before, after = (x.shape[:dim], x.shape[dim + 1 :])
    return jnp.moveaxis(x.reshape(*before, peers, -1, *after), dim, 0)


def sent_and_summed(x, axis, dim):
    tiles = in_blocks(x, dim, lax.axis_size(axis))
    arrived = lax.all_to_all(tiles, axis, split_axis=0, concat_axis=0, tiled=True)
    return arrived.astype(jnp.float32).sum(axis=0)


def copy_for_each(x, axis):
    copies = jnp.broadcast_to(x, (lax.axis_size(axis), *x.shape))
    return lax.all_to_all(copies, axis, split_axis=0, concat_axis=0, tiled=True)


def of_everyone(x, axis):
    return copy_for_each(x, axis).sum(axis=0)


def rotate(projected, position):
    half_width = projected.shape[-1] // 2
    inverse = 1.0 / 10000.0 ** jnp.linspace(0.0, 1.0, half_width, dtype=jnp.float32)
    angle = position[:, None] * inverse[None, :]
    cosine = jnp.cos(angle)[:, None, :]
    sine = jnp.sin(angle)[:, None, :]
    first = projected[..., :half_width]
    second = projected[..., half_width:]
    return jnp.concatenate(
        [first * cosine - second * sine, first * sine + second * cosine], axis=-1
    )


def on_device(
    layer_input, key_weight, value_weight, decay_exponent, query_new, key_new, value_new, norm_gain
):
    tok_count = layer_input.shape[0]
    head_local = decay_exponent.shape[0]
    key_width = key_weight.shape[1] // head_local
    value_width = value_weight.shape[1] // head_local
    seq_span = lax.axis_size("sp") // SEQS
    seq_length = tok_count * seq_span
    sp_place = lax.axis_index("sp")
    feature_block = lax.all_gather(layer_input, "tp", axis=1, tiled=True)
    key_proj = jnp.dot(feature_block, key_weight, preferred_element_type=jnp.float32)
    value_proj = jnp.dot(feature_block, value_weight, preferred_element_type=jnp.float32)
    position = (sp_place % seq_span * tok_count + jnp.arange(tok_count, dtype=jnp.int32)).astype(
        jnp.float32
    )
    keys = (
        rotate(key_proj.reshape(tok_count, head_local, key_width), position) * key_width ** (-0.5)
    ).astype(jnp.bfloat16)
    values = value_proj.astype(jnp.bfloat16).reshape(tok_count, head_local, value_width)
    distance = seq_length - 1.0 - position
    weighting = jnp.exp(decay_exponent[None, :] * distance[:, None])
    weighted = (keys.astype(jnp.float32) * weighting[:, :, None]).astype(jnp.bfloat16)
    local_state = jnp.einsum("thd,the->hde", weighted, values, preferred_element_type=jnp.float32)
    member = (jnp.arange(SEQS, dtype=jnp.int32) == sp_place // seq_span).astype(jnp.float32)
    state_terms = member[:, None, None, None] * local_state[None]
    final_rows = sent_and_summed(state_terms.astype(jnp.bfloat16), "sp", 2)
    state_cache = final_rows.astype(jnp.bfloat16)
    queries = query_new.astype(jnp.float32).reshape(SEQS, head_local, key_width)
    partial_read = jnp.einsum(
        "shd,shde->she", queries, state_terms, precision=lax.Precision.HIGHEST
    )
    carried = of_everyone(partial_read, "sp")
    keys_next = key_new.astype(jnp.float32).reshape(SEQS, head_local, key_width)
    values_next = value_new.astype(jnp.float32).reshape(SEQS, head_local, value_width)
    own_term = jnp.sum(queries * keys_next, axis=2)[:, :, None] * values_next
    mixed = jnp.exp(decay_exponent)[None, :, None] * carried + own_term
    normed = mixed * lax.rsqrt(jnp.mean(mixed * mixed, axis=2, keepdims=True) + 1e-06)
    normed = normed * norm_gain.reshape(head_local, value_width)[None, :, :]
    return (state_cache, normed.reshape(SEQS, head_local * value_width).astype(jnp.bfloat16))


def solution(mesh):
    in_specs = (
        P("sp", "tp"),
        P(None, "tp"),
        P(None, "tp"),
        P("tp"),
        P(None, "tp"),
        P(None, "tp"),
        P(None, "tp"),
        P("tp"),
    )
    out_specs = (P(None, "tp", "sp", None), P(None, "tp"))
    return jax.shard_map(
        on_device, mesh=mesh, in_specs=in_specs, out_specs=out_specs, check_vma=False
    )
```

profile of v0, /device:TPU:1, one launch (start us, length us, event | category | flops | bytes accessed | tf_op | source)
XLA Modules:
  0.0 174.9 jit_solution(16979299565072083331)
XLA Ops:
  7.2 0.7 all-gather.2.cloned.1.call-update
  7.9 0.7 reshape.155
  8.6 0.7 exp.11
  9.3 0.1 fusion.12
  9.4 0.7 convert_multiply_fusion
  10.1 0.7 multiply_exponential_fusion
  10.8 1.0 multiply_cosine_fusion
  11.8 95.6 %all-gather.2.cloned.1.call-done = bf16[1024,4096]{1,0:T(8,128)(2,1)} async-done(((bf16[1024,256]{1,0:T(8,128)(2,1)}), bf16[1024,4096]{1,0:T(8,128)(2,1)}) %all-gather.2.cloned.1.call-update) | async-done | bytes 8388624 | tf_op jit(solution)/shard_map/all_gather | solution.py:52
  107.5 5.9 %fusion.15 = f32[1024,256]{0,1:T(8,128)S(1)} fusion(bf16[1024,4096]{1,0:T(8,128)(2,1)} %all-gather.2.cloned.1.call-done, bf16[4096,256]{1,0:T(8,128)(2,1)S(1)} %copy-done), kind=kOutput, calls=%fused_computation.37 | convolution fusion | flops 2147483648 | bytes 11534336 | tf_op jit(solution)/shard_map/dot_general | solution.py:53
  113.4 0.2 multiply_subtract_fusion
  113.6 1.4 copy-done.4
  115.0 2.4 %convolution_convert_fusion = bf16[1024,256]{0,1:T(8,128)(2,1)S(1)} fusion(bf16[1024,4096]{1,0:T(8,128)(2,1)S(1)} %copy-done.3, bf16[4096,256]{1,0:T(8,128)(2,1)S(1)} %copy-done.4), kind=kOutput, calls=%fused_computation | convolution fusion | flops 2147745792 | bytes 11010048 | tf_op jit(solution)/shard_map/dot_general | solution.py:54
  117.4 0.3 fusion.1
  117.7 0.3 fusion.5
  118.0 0.6 broadcast_in_dim.4
  118.7 14.4 %all-to-all-start.1 = ((f32[32,2,2,128]{3,2,1,0:T(2,128)}), f32[32,2,2,128]{3,2,1,0:T(2,128)S(1)}, u32[]{:S(2)}, u32[]{:S(2)}) async-start(f32[32,2,2,128]{3,2,1,0:T(2,128)} %broadcast_in_dim.4), calls=%async_computation.1 | async-start | bytes 131072 | tf_op jit(solution)/shard_map/all_to_all | solution.py:22
  133.2 0.1 reduce_sum.44
  133.2 0.8 multiply_convert_fusion.2
  134.0 12.1 %all-to-all-done.1 = f32[32,2,2,128]{3,2,1,0:T(2,128)S(1)} async-done(((f32[32,2,2,128]{3,2,1,0:T(2,128)}), f32[32,2,2,128]{3,2,1,0:T(2,128)S(1)}, u32[]{:S(2)}, u32[]{:S(2)}) %all-to-all-start.1) | async-done | bytes 65568 | tf_op jit(solution)/shard_map/all_to_all | solution.py:22
  146.1 5.1 %all-to-all-start = ((bf16[32,2,2,4,128]{4,3,2,1,0:T(4,128)(2,1)}), bf16[32,2,2,4,128]{4,3,2,1,0:T(4,128)(2,1)S(1)}, u32[]{:S(2)}, u32[]{:S(2)}) async-start(bf16[32,2,2,4,128]{4,3,2,1,0:T(4,128)(2,1)} %multiply_convert_fusion.2), calls=%async_computation | async-start | bytes 262144 | tf_op jit(solution)/shard_map/all_to_all | solution.py:16
  151.2 0.2 broadcast_bitcast_fusion.1
  151.5 0.6 fusion.10
  152.0 15.3 %all-to-all-done = bf16[32,2,2,4,128]{4,3,2,1,0:T(4,128)(2,1)S(1)} async-done(((bf16[32,2,2,4,128]{4,3,2,1,0:T(4,128)(2,1)}), bf16[32,2,2,4,128]{4,3,2,1,0:T(4,128)(2,1)S(1)}, u32[]{:S(2)}, u32[]{:S(2)}) %all-to-all-start) | async-done | bytes 131104 | tf_op jit(solution)/shard_map/all_to_all | solution.py:16
  167.4 0.7 reduce_sum.41
  (20 shorter events, 0.3 us)
Async XLA Ops:
  7.2 100.3 %copy-start = (bf16[4096,256]{1,0:T(8,128)(2,1)S(1)}, bf16[4096,256]{1,0:T(8,128)(2,1)}, u32[]{:S(2)}) copy-start(bf16[4096,256]{1,0:T(8,128)(2,1)} %param.9) | copy-start | bytes 6291460
  7.2 100.3 %all-gather.2.cloned.1.call-start = ((), (), s32[]{:S(2)}) async-start(), calls=%async_computation.2 | async-start | bytes 8912896 | tf_op jit(solution)/shard_map/all_gather | solution.py:52
  107.5 6.1 %copy-start.3 = (bf16[1024,4096]{1,0:T(8,128)(2,1)S(1)}, bf16[1024,4096]{1,0:T(8,128)(2,1)}, u32[]{:S(2)}) copy-start(bf16[1024,4096]{1,0:T(8,128)(2,1)} %all-gather.2.cloned.1.call-done) | copy-start | bytes 25165828
  113.4 1.6 copy-start.4
  117.4 15.8 %copy-start.1 = (bf16[2,256]{1,0:T(2,128)(2,1)S(1)}, bf16[2,256]{1,0:T(2,128)(2,1)}, u32[]{:S(2)}) copy-start(bf16[2,256]{1,0:T(2,128)(2,1)} %param.14) | copy-start | bytes 3076
  117.4 34.1 %copy-start.2 = (f32[256]{0:T(256)S(1)}, f32[256]{0:T(256)}, u32[]{:S(2)}) copy-start(f32[256]{0:T(256)} %param.15) | copy-start | bytes 3076
  118.7 27.4 %all-to-all-start.1 = ((f32[32,2,2,128]{3,2,1,0:T(2,128)}), f32[32,2,2,128]{3,2,1,0:T(2,128)S(1)}, u32[]{:S(2)}, u32[]{:S(2)}) async-start(f32[32,2,2,128]{3,2,1,0:T(2,128)} %broadcast_in_dim.4), calls=%async_computation.1 | async-start | bytes 131072 | tf_op jit(solution)/shard_map/all_to_all | solution.py:22
  146.1 21.3 %all-to-all-start = ((bf16[32,2,2,4,128]{4,3,2,1,0:T(4,128)(2,1)}), bf16[32,2,2,4,128]{4,3,2,1,0:T(4,128)(2,1)S(1)}, u32[]{:S(2)}, u32[]{:S(2)}) async-start(bf16[32,2,2,4,128]{4,3,2,1,0:T(4,128)(2,1)} %multiply_convert_fusion.2), calls=%async_computation | async-start | bytes 262144 | tf_op jit(solution)/shard_map/all_to_all | solution.py:16
Sparse Core Ops, SparseCore 0:
  11.0 96.4 all-gather.1
where the time goes:
time: 175 us
  waiting for transfers between devices  124 us (71%)
  starting transfers between devices  19.5 us (11%)
  between operations  14.2 us (8%)
  matrix products  8.92 us (5%)
  other arithmetic  4.99 us (3%)
  local copies, waits for them, and re-layouts  3.61 us (2%)
    all_gather x1, waiting for transfers between devices, on_device(): feature_block = lax.all_gather(layer_input, 'tp', axis=1, tiled=True)  95.6 us
    all_to_all x1, waiting for transfers between devices, sent_and_summed(): lax.all_to_all(tiles, axis, split_axis=0, concat_axis=0, tiled=True)  15.3 us
    all_to_all x1, starting transfers between devices, copy_for_each(): return lax.all_to_all(copies, axis, split_axis=0, concat_axis=0, tiled=True)  14.4 us
    all_to_all x1, waiting for transfers between devices, copy_for_each(): return lax.all_to_all(copies, axis, split_axis=0, concat_axis=0, tiled=True)  12.1 us
    dot_general x1, matrix products, on_device(): jnp.dot(feature_block, key_weight, preferred_element_type=jnp.float32)  5.9 us
    all_to_all x1, starting transfers between devices, sent_and_summed(): lax.all_to_all(tiles, axis, split_axis=0, concat_axis=0, tiled=True)  5.1 us
  transfers between devices with their start and end apart: 3, of which 3 were waited for; matrix products, arithmetic and copies ran while one was open for 3% of the time, Pallas kernels for 0%

commit v1 on v0

--- a/solution.py
+++ b/solution.py
@@ -49,7 +49,27 @@
     seq_span = lax.axis_size("sp") // SEQS
     seq_length = tok_count * seq_span
     sp_place = lax.axis_index("sp")
-    feature_block = lax.all_gather(layer_input, "tp", axis=1, tiled=True)
+    size, index, rows = (lax.axis_size("tp"), lax.axis_index("tp"), layer_input.shape[1])
+    ahead = [(i, (i + 1) % size) for i in range(size)]
+    downward = [(i, (i - 1) % size) for i in range(size)]
+    feature_block = jnp.zeros(
+        (*layer_input.shape[:1], size * rows, *layer_input.shape[1 + 1 :]), layer_input.dtype
+    )
+    feature_block = lax.dynamic_update_slice_in_dim(
+        feature_block, layer_input, index * rows, axis=1
+    )
+    from_left = from_right = layer_input
+    middle = size // 2
+    for step in range(1, middle + 1):
+        from_left = lax.ppermute(from_left, "tp", ahead)
+        feature_block = lax.dynamic_update_slice_in_dim(
+            feature_block, from_left, (index - step) % size * rows, axis=1
+        )
+        if step < size - middle:
+            from_right = lax.ppermute(from_right, "tp", downward)
+            feature_block = lax.dynamic_update_slice_in_dim(
+                feature_block, from_right, (index + step) % size * rows, axis=1
+            )
     key_proj = jnp.dot(feature_block, key_weight, preferred_element_type=jnp.float32)
     value_proj = jnp.dot(feature_block, value_weight, preferred_element_type=jnp.float32)
     position = (sp_place % seq_span * tok_count + jnp.arange(tok_count, dtype=jnp.int32)).astype(

time: 175 us -> 206 us (1.18)
  starting transfers between devices: 19.5 us -> 105 us
  waiting for transfers between devices: 124 us -> 51 us
  local copies, waits for them, and re-layouts: 3.61 us -> 29.8 us
  between operations: 14.2 us -> 1.31 us
  matrix products: 8.92 us -> 12.3 us
    all_gather x1 -> x0, waiting for transfers between devices: 95.6 us -> none  [on_device(): feature_block = lax.all_gather(layer_input, 'tp', axis=1, tiled=True)]
    ppermute x0 -> x15, starting transfers between devices: none -> 65.7 us  [the longest x7 45.6 us: on_device(): from_right = lax.ppermute(from_right, 'tp', downward)]
    dynamic_update_slice x0 -> x16, local copies, waits for them, and re-layouts: none -> 24.6 us  [the longest x8 12.3 us: on_device(): lax.dynamic_update_slice_in_dim(feature_block, from_left, (index - step)...]
    ppermute x0 -> x15, waiting for transfers between devices: none -> 23.6 us  [the longest x8 23.5 us: on_device(): from_left = lax.ppermute(from_left, 'tp', ahead)]
    all_to_all x1, starting transfers between devices: 14.4 us -> 34.5 us  [copy_for_each(): return lax.all_to_all(copies, axis, split_axis=0, concat_axis=0, tiled=True)]
    broadcast_in_dim x0 -> x1, local copies, waits for them, and re-layouts: none -> 4.29 us  [on_device(): jnp.zeros((*layer_input.shape[:1], size * rows, *layer_input.shape[1 + 1:...]
    dot_general x1, matrix products: 2.41 us -> 5.78 us  [on_device(): jnp.dot(feature_block, value_weight, preferred_element_type=jnp.float32)]
  transfers between devices with their start and end apart: 3 -> 17, of which waited for: 3 -> 8; matrix products, arithmetic and copies ran while one was open for 3% -> 16% of each run, Pallas kernels for 0% -> 0%
where the time goes in v1:
time: 206 us; the launch traced here: 205 us
  starting transfers between devices  105 us (51%)
  waiting for transfers between devices  51 us (25%)
  local copies, waits for them, and re-layouts  29.8 us (14%)
  matrix products  12.3 us (6%)
  other arithmetic  5 us (2%)
    ppermute x7, starting transfers between devices, on_device(): from_right = lax.ppermute(from_right, 'tp', downward)  45.6 us
    all_to_all x1, starting transfers between devices, copy_for_each(): return lax.all_to_all(copies, axis, split_axis=0, concat_axis=0, tiled=True)  34.5 us
    ppermute x8, waiting for transfers between devices, on_device(): from_left = lax.ppermute(from_left, 'tp', ahead)  23.5 us
    ppermute x8, starting transfers between devices, on_device(): from_left = lax.ppermute(from_left, 'tp', ahead)  20 us
    all_to_all x1, waiting for transfers between devices, sent_and_summed(): lax.all_to_all(tiles, axis, split_axis=0, concat_axis=0, tiled=True)  15.3 us
    dynamic_update_slice x8, local copies, waits for them, and re-layouts, on_device(): lax.dynamic_update_slice_in_dim(feature_block, from_left, (index - step)...  12.3 us
    all_to_all x1, waiting for transfers between devices, copy_for_each(): return lax.all_to_all(copies, axis, split_axis=0, concat_axis=0, tiled=True)  12.1 us
    dynamic_update_slice x7, local copies, waits for them, and re-layouts, on_device(): lax.dynamic_update_slice_in_dim(feature_block, from_right, (index + step)...  11.4 us
  transfers between devices with their start and end apart: 17, of which 8 were waited for; matrix products, arithmetic and copies ran while one was open for 16% of the time, Pallas kernels for 0%

profile of v1, /device:TPU:1, one launch (start us, length us, event | category | flops | bytes accessed | tf_op | source)
XLA Modules:
  0.0 204.6 jit_solution(9694322404143259579)
XLA Ops:
  0.7 4.1 %collective-permute-start = (bf16[1024,256]{1,0:T(8,128)(2,1)}, bf16[1024,256]{1,0:T(8,128)(2,1)S(1)}, u32[]{:S(2)}, u32[]{:S(2)}) collective-permute-start(bf16[1024,256]{1,0:T(8,128)(2,1)} %param.8), channel_id=1, source_target_pairs={{0,1},{1,2},{2,3},{3,4},{4,5},{5,6},{6,7},{7,8},{8,9},{9,10},{10,1... | collective-permute-start | bytes 1572872 | tf_op jit(solution)/shard_map/ppermute | solution.py:64
  4.8 5.6 %collective-permute-start.1 = (bf16[1024,256]{1,0:T(8,128)(2,1)}, bf16[1024,256]{1,0:T(8,128)(2,1)}, u32[]{:S(2)}, u32[]{:S(2)}) collective-permute-start(bf16[1024,256]{1,0:T(8,128)(2,1)} %param.8), channel_id=1, source_target_pairs={{0,15},{1,0},{2,1},{3,2},{4,3},{5,4},{6,5},{7,6},{8,7},{9,8},{10,9... | collective-permute-start | bytes 1572872 | tf_op jit(solution)/shard_map/ppermute | solution.py:69
  10.4 4.8 %collective-permute-done = bf16[1024,256]{1,0:T(8,128)(2,1)S(1)} collective-permute-done((bf16[1024,256]{1,0:T(8,128)(2,1)}, bf16[1024,256]{1,0:T(8,128)(2,1)S(1)}, u32[]{:S(2)}, u32[]{:S(2)}) %collective-permute-start) | collective-permute-done | bytes 524320 | tf_op jit(solution)/shard_map/ppermute | solution.py:64
  15.2 3.5 %collective-permute-start.2 = (bf16[1024,256]{1,0:T(8,128)(2,1)S(1)}, bf16[1024,256]{1,0:T(8,128)(2,1)}, u32[]{:S(2)}, u32[]{:S(2)}) collective-permute-start(bf16[1024,256]{1,0:T(8,128)(2,1)S(1)} %collective-permute-done), channel_id=1, source_target_pairs={{0,1},{1,2},{2,3},{3,4},{4,5},{5,6},{6,7},{7,8},{8,9},{9,10},{10,1... | collective-permute-start | bytes 1572872 | tf_op jit(solution)/shard_map/ppermute | solution.py:64
  18.8 6.5 %collective-permute-start.3 = (bf16[1024,256]{1,0:T(8,128)(2,1)}, bf16[1024,256]{1,0:T(8,128)(2,1)}, u32[]{:S(2)}, u32[]{:S(2)}) collective-permute-start(bf16[1024,256]{1,0:T(8,128)(2,1)} %collective-permute-done.1), channel_id=1, source_target_pairs={{0,15},{1,0},{2,1},{3,2},{4,3},{5,4},{6,5},{7,6},{8,7},{9,8},{10,9... | collective-permute-start | bytes 1572872 | tf_op jit(solution)/shard_map/ppermute | solution.py:69
  25.3 4.7 %collective-permute-done.2 = bf16[1024,256]{1,0:T(8,128)(2,1)} collective-permute-done((bf16[1024,256]{1,0:T(8,128)(2,1)S(1)}, bf16[1024,256]{1,0:T(8,128)(2,1)}, u32[]{:S(2)}, u32[]{:S(2)}) %collective-permute-start.2) | collective-permute-done | bytes 524320 | tf_op jit(solution)/shard_map/ppermute | solution.py:64
  30.0 2.7 %collective-permute-start.4 = (bf16[1024,256]{1,0:T(8,128)(2,1)}, bf16[1024,256]{1,0:T(8,128)(2,1)S(1)}, u32[]{:S(2)}, u32[]{:S(2)}) collective-permute-start(bf16[1024,256]{1,0:T(8,128)(2,1)} %collective-permute-done.2), channel_id=1, source_target_pairs={{0,1},{1,2},{2,3},{3,4},{4,5},{5,6},{6,7},{7,8},{8,9},{9,10},{10,1... | collective-permute-start | bytes 1572872 | tf_op jit(solution)/shard_map/ppermute | solution.py:64
  32.7 6.5 %collective-permute-start.5 = (bf16[1024,256]{1,0:T(8,128)(2,1)}, bf16[1024,256]{1,0:T(8,128)(2,1)}, u32[]{:S(2)}, u32[]{:S(2)}) collective-permute-start(bf16[1024,256]{1,0:T(8,128)(2,1)} %collective-permute-done.3), channel_id=1, source_target_pairs={{0,15},{1,0},{2,1},{3,2},{4,3},{5,4},{6,5},{7,6},{8,7},{9,8},{10,9... | collective-permute-start | bytes 1572872 | tf_op jit(solution)/shard_map/ppermute | solution.py:69
  39.3 4.8 %collective-permute-done.4 = bf16[1024,256]{1,0:T(8,128)(2,1)S(1)} collective-permute-done((bf16[1024,256]{1,0:T(8,128)(2,1)}, bf16[1024,256]{1,0:T(8,128)(2,1)S(1)}, u32[]{:S(2)}, u32[]{:S(2)}) %collective-permute-start.4) | collective-permute-done | bytes 524320 | tf_op jit(solution)/shard_map/ppermute | solution.py:64
  44.1 2.1 %collective-permute-start.6 = (bf16[1024,256]{1,0:T(8,128)(2,1)S(1)}, bf16[1024,256]{1,0:T(8,128)(2,1)}, u32[]{:S(2)}, u32[]{:S(2)}) collective-permute-start(bf16[1024,256]{1,0:T(8,128)(2,1)S(1)} %collective-permute-done.4), channel_id=1, source_target_pairs={{0,1},{1,2},{2,3},{3,4},{4,5},{5,6},{6,7},{7,8},{8,9},{9,10},{10,1... | collective-permute-start | bytes 1572872 | tf_op jit(solution)/shard_map/ppermute | solution.py:64
  47.7 6.5 %collective-permute-start.7 = (bf16[1024,256]{1,0:T(8,128)(2,1)}, bf16[1024,256]{1,0:T(8,128)(2,1)}, u32[]{:S(2)}, u32[]{:S(2)}) collective-permute-start(bf16[1024,256]{1,0:T(8,128)(2,1)} %collective-permute-done.5), channel_id=1, source_target_pairs={{0,15},{1,0},{2,1},{3,2},{4,3},{5,4},{6,5},{7,6},{8,7},{9,8},{10,9... | collective-permute-start | bytes 1572872 | tf_op jit(solution)/shard_map/ppermute | solution.py:69
  54.2 3.3 %collective-permute-done.6 = bf16[1024,256]{1,0:T(8,128)(2,1)} collective-permute-done((bf16[1024,256]{1,0:T(8,128)(2,1)S(1)}, bf16[1024,256]{1,0:T(8,128)(2,1)}, u32[]{:S(2)}, u32[]{:S(2)}) %collective-permute-start.6) | collective-permute-done | bytes 524320 | tf_op jit(solution)/shard_map/ppermute | solution.py:64
  60.6 7.1 %collective-permute-start.9 = (bf16[1024,256]{1,0:T(8,128)(2,1)}, bf16[1024,256]{1,0:T(8,128)(2,1)}, u32[]{:S(2)}, u32[]{:S(2)}) collective-permute-start(bf16[1024,256]{1,0:T(8,128)(2,1)} %collective-permute-done.7), channel_id=1, source_target_pairs={{0,15},{1,0},{2,1},{3,2},{4,3},{5,4},{6,5},{7,6},{8,7},{9,8},{10,9... | collective-permute-start | bytes 1572872 | tf_op jit(solution)/shard_map/ppermute | solution.py:69
  67.7 4.3 %broadcast_in_dim.6 = bf16[1024,4096]{1,0:T(8,128)(2,1)} broadcast(bf16[]{:T(256)} %constant.131.clone.1), dimensions={} | broadcast | bytes 8388610 | tf_op jit(solution)/shard_map/broadcast_in_dim | solution.py:55
  79.0 2.0 constant_dynamic-update-slice_fusion.12
  81.0 6.7 %collective-permute-start.11 = (bf16[1024,256]{1,0:T(8,128)(2,1)}, bf16[1024,256]{1,0:T(8,128)(2,1)S(1)}, u32[]{:S(2)}, u32[]{:S(2)}) collective-permute-start(bf16[1024,256]{1,0:T(8,128)(2,1)} %collective-permute-done.9), channel_id=1, source_target_pairs={{0,15},{1,0},{2,1},{3,2},{4,3},{5,4},{6,5},{7,6},{8,7},{9,8},{10,9... | collective-permute-start | bytes 1572872 | tf_op jit(solution)/shard_map/ppermute | solution.py:69
  99.3 6.7 %collective-permute-start.13 = (bf16[1024,256]{1,0:T(8,128)(2,1)S(1)}, bf16[1024,256]{1,0:T(8,128)(2,1)S(1)}, u32[]{:S(2)}, u32[]{:S(2)}) collective-permute-start(bf16[1024,256]{1,0:T(8,128)(2,1)S(1)} %collective-permute-done.11), channel_id=1, source_target_pairs={{0,15},{1,0},{2,1},{3,2},{4,3},{5,4},{6,5},{7,6},{8,7},{9,8},{10,9... | collective-permute-start | bytes 1572872 | tf_op jit(solution)/shard_map/ppermute | solution.py:69
  115.2 5.9 %collective-permute-done.14 = bf16[1024,256]{1,0:T(8,128)(2,1)S(1)} collective-permute-done((bf16[1024,256]{1,0:T(8,128)(2,1)S(1)}, bf16[1024,256]{1,0:T(8,128)(2,1)S(1)}, u32[]{:S(2)}, u32[]{:S(2)}) %collective-permute-start.14) | collective-permute-done | bytes 524320 | tf_op jit(solution)/shard_map/ppermute | solution.py:64
  122.0 5.9 %fusion.15 = f32[1024,256]{0,1:T(8,128)S(1)} fusion(bf16[1024,4096]{1,0:T(8,128)(2,1)} %constant_dynamic-update-slice_fusion, bf16[4096,256]{1,0:T(8,128)(2,1)S(1)} %copy-done), kind=kOutput, calls=%fused_computation.53 | convolution fusion | flops 2147483648 | bytes 11534336 | tf_op jit(solution)/shard_map/dot_general | solution.py:73
  127.9 5.8 %convolution_convert_fusion = bf16[1024,256]{0,1:T(8,128)(2,1)S(1)} fusion(bf16[1024,4096]{1,0:T(8,128)(2,1)} %constant_dynamic-update-slice_fusion, bf16[4096,256]{1,0:T(8,128)(2,1)S(1)} %copy-done.8), kind=kOutput, calls=%fused_computation | convolution fusion | flops 2147745792 | bytes 11010048 | tf_op jit(solution)/shard_map/dot_general | solution.py:74
  135.2 34.5 %all-to-all-start.1 = ((f32[32,2,2,128]{3,2,1,0:T(2,128)}), f32[32,2,2,128]{3,2,1,0:T(2,128)S(1)}, u32[]{:S(2)}, u32[]{:S(2)}) async-start(f32[32,2,2,128]{3,2,1,0:T(2,128)} %broadcast_in_dim.7), calls=%async_computation.1 | async-start | bytes 131072 | tf_op jit(solution)/shard_map/all_to_all | solution.py:22
  170.6 12.1 %all-to-all-done.1 = f32[32,2,2,128]{3,2,1,0:T(2,128)S(1)} async-done(((f32[32,2,2,128]{3,2,1,0:T(2,128)}), f32[32,2,2,128]{3,2,1,0:T(2,128)S(1)}, u32[]{:S(2)}, u32[]{:S(2)}) %all-to-all-start.1) | async-done | bytes 65568 | tf_op jit(solution)/shard_map/all_to_all | solution.py:22
  182.6 5.1 %all-to-all-start = ((bf16[32,2,2,4,128]{4,3,2,1,0:T(4,128)(2,1)}), bf16[32,2,2,4,128]{4,3,2,1,0:T(4,128)(2,1)S(1)}, u32[]{:S(2)}, u32[]{:S(2)}) async-start(bf16[32,2,2,4,128]{4,3,2,1,0:T(4,128)(2,1)} %multiply_convert_fusion.2), calls=%async_computation | async-start | bytes 262144 | tf_op jit(solution)/shard_map/all_to_all | solution.py:16
  188.6 15.3 %all-to-all-done = bf16[32,2,2,4,128]{4,3,2,1,0:T(4,128)(2,1)S(1)} async-done(((bf16[32,2,2,4,128]{4,3,2,1,0:T(4,128)(2,1)}), bf16[32,2,2,4,128]{4,3,2,1,0:T(4,128)(2,1)S(1)}, u32[]{:S(2)}, u32[]{:S(2)}) %all-to-all-start) | async-done | bytes 131104 | tf_op jit(solution)/shard_map/all_to_all | solution.py:16
  (72 shorter events, 37.0 us)
Async XLA Ops:
  0.6 121.4 %copy-start = (bf16[4096,256]{1,0:T(8,128)(2,1)S(1)}, bf16[4096,256]{1,0:T(8,128)(2,1)}, u32[]{:S(2)}) copy-start(bf16[4096,256]{1,0:T(8,128)(2,1)} %param.9) | copy-start | bytes 6291460
  0.6 71.3 %copy-start.1 = (bf16[1024,256]{1,0:T(8,128)(2,1)S(1)}, bf16[1024,256]{1,0:T(8,128)(2,1)}, u32[]{:S(2)}) copy-start(bf16[1024,256]{1,0:T(8,128)(2,1)} %param.8) | copy-start | bytes 1572868
  0.7 74.4 %copy-start.5 = (bf16[2,256]{1,0:T(2,128)(2,1)S(1)}, bf16[2,256]{1,0:T(2,128)(2,1)}, u32[]{:S(2)}) copy-start(bf16[2,256]{1,0:T(2,128)(2,1)} %param.12) | copy-start | bytes 3076
  0.7 74.4 %copy-start.7 = (f32[2]{0:T(128)S(1)}, f32[2]{0:T(128)}, u32[]{:S(2)}) copy-start(f32[2]{0:T(128)} %param.11) | copy-start | bytes 28
  0.7 14.6 %collective-permute-start = (bf16[1024,256]{1,0:T(8,128)(2,1)}, bf16[1024,256]{1,0:T(8,128)(2,1)S(1)}, u32[]{:S(2)}, u32[]{:S(2)}) collective-permute-start(bf16[1024,256]{1,0:T(8,128)(2,1)} %param.8), channel_id=1, source_target_pairs={{0,1},{1,2},{2,3},{3,4},{4,5},{5,6},{6,7},{7,8},{8,9},{9,10},{10,1... | collective-permute-start | bytes 1572872 | tf_op jit(solution)/shard_map/ppermute | solution.py:64
  4.8 14.0 %collective-permute-start.1 = (bf16[1024,256]{1,0:T(8,128)(2,1)}, bf16[1024,256]{1,0:T(8,128)(2,1)}, u32[]{:S(2)}, u32[]{:S(2)}) collective-permute-start(bf16[1024,256]{1,0:T(8,128)(2,1)} %param.8), channel_id=1, source_target_pairs={{0,15},{1,0},{2,1},{3,2},{4,3},{5,4},{6,5},{7,6},{8,7},{9,8},{10,9... | collective-permute-start | bytes 1572872 | tf_op jit(solution)/shard_map/ppermute | solution.py:69
  15.2 14.8 %collective-permute-start.2 = (bf16[1024,256]{1,0:T(8,128)(2,1)S(1)}, bf16[1024,256]{1,0:T(8,128)(2,1)}, u32[]{:S(2)}, u32[]{:S(2)}) collective-permute-start(bf16[1024,256]{1,0:T(8,128)(2,1)S(1)} %collective-permute-done), channel_id=1, source_target_pairs={{0,1},{1,2},{2,3},{3,4},{4,5},{5,6},{6,7},{7,8},{8,9},{9,10},{10,1... | collective-permute-start | bytes 1572872 | tf_op jit(solution)/shard_map/ppermute | solution.py:64
  18.8 13.9 %collective-permute-start.3 = (bf16[1024,256]{1,0:T(8,128)(2,1)}, bf16[1024,256]{1,0:T(8,128)(2,1)}, u32[]{:S(2)}, u32[]{:S(2)}) collective-permute-start(bf16[1024,256]{1,0:T(8,128)(2,1)} %collective-permute-done.1), channel_id=1, source_target_pairs={{0,15},{1,0},{2,1},{3,2},{4,3},{5,4},{6,5},{7,6},{8,7},{9,8},{10,9... | collective-permute-start | bytes 1572872 | tf_op jit(solution)/shard_map/ppermute | solution.py:69
  30.0 14.0 %collective-permute-start.4 = (bf16[1024,256]{1,0:T(8,128)(2,1)}, bf16[1024,256]{1,0:T(8,128)(2,1)S(1)}, u32[]{:S(2)}, u32[]{:S(2)}) collective-permute-start(bf16[1024,256]{1,0:T(8,128)(2,1)} %collective-permute-done.2), channel_id=1, source_target_pairs={{0,1},{1,2},{2,3},{3,4},{4,5},{5,6},{6,7},{7,8},{8,9},{9,10},{10,1... | collective-permute-start | bytes 1572872 | tf_op jit(solution)/shard_map/ppermute | solution.py:64
  32.7 14.9 %collective-permute-start.5 = (bf16[1024,256]{1,0:T(8,128)(2,1)}, bf16[1024,256]{1,0:T(8,128)(2,1)}, u32[]{:S(2)}, u32[]{:S(2)}) collective-permute-start(bf16[1024,256]{1,0:T(8,128)(2,1)} %collective-permute-done.3), channel_id=1, source_target_pairs={{0,15},{1,0},{2,1},{3,2},{4,3},{5,4},{6,5},{7,6},{8,7},{9,8},{10,9... | collective-permute-start | bytes 1572872 | tf_op jit(solution)/shard_map/ppermute | solution.py:69
  44.1 15.3 %copy-start.2 = (bf16[1024,256]{1,0:T(8,128)(2,1)}, bf16[1024,256]{1,0:T(8,128)(2,1)S(1)}, u32[]{:S(2)}) copy-start(bf16[1024,256]{1,0:T(8,128)(2,1)S(1)} %collective-permute-done.4) | copy-start | bytes 1572868
  44.1 13.3 %collective-permute-start.6 = (bf16[1024,256]{1,0:T(8,128)(2,1)S(1)}, bf16[1024,256]{1,0:T(8,128)(2,1)}, u32[]{:S(2)}, u32[]{:S(2)}) collective-permute-start(bf16[1024,256]{1,0:T(8,128)(2,1)S(1)} %collective-permute-done.4), channel_id=1, source_target_pairs={{0,1},{1,2},{2,3},{3,4},{4,5},{5,6},{6,7},{7,8},{8,9},{9,10},{10,1... | collective-permute-start | bytes 1572872 | tf_op jit(solution)/shard_map/ppermute | solution.py:64
  47.7 12.9 %collective-permute-start.7 = (bf16[1024,256]{1,0:T(8,128)(2,1)}, bf16[1024,256]{1,0:T(8,128)(2,1)}, u32[]{:S(2)}, u32[]{:S(2)}) collective-permute-start(bf16[1024,256]{1,0:T(8,128)(2,1)} %collective-permute-done.5), channel_id=1, source_target_pairs={{0,15},{1,0},{2,1},{3,2},{4,3},{5,4},{6,5},{7,6},{8,7},{9,8},{10,9... | collective-permute-start | bytes 1572872 | tf_op jit(solution)/shard_map/ppermute | solution.py:69
  57.4 15.4 %collective-permute-start.8 = (bf16[1024,256]{1,0:T(8,128)(2,1)}, bf16[1024,256]{1,0:T(8,128)(2,1)}, u32[]{:S(2)}, u32[]{:S(2)}) collective-permute-start(bf16[1024,256]{1,0:T(8,128)(2,1)} %collective-permute-done.6), channel_id=1, source_target_pairs={{0,1},{1,2},{2,3},{3,4},{4,5},{5,6},{6,7},{7,8},{8,9},{9,10},{10,1... | collective-permute-start | bytes 1572872 | tf_op jit(solution)/shard_map/ppermute | solution.py:64
  60.6 20.4 %collective-permute-start.9 = (bf16[1024,256]{1,0:T(8,128)(2,1)}, bf16[1024,256]{1,0:T(8,128)(2,1)}, u32[]{:S(2)}, u32[]{:S(2)}) collective-permute-start(bf16[1024,256]{1,0:T(8,128)(2,1)} %collective-permute-done.7), channel_id=1, source_target_pairs={{0,15},{1,0},{2,1},{3,2},{4,3},{5,4},{6,5},{7,6},{8,7},{9,8},{10,9... | collective-permute-start | bytes 1572872 | tf_op jit(solution)/shard_map/ppermute | solution.py:69
  72.9 16.8 %collective-permute-start.10 = (bf16[1024,256]{1,0:T(8,128)(2,1)}, bf16[1024,256]{1,0:T(8,128)(2,1)S(1)}, u32[]{:S(2)}, u32[]{:S(2)}) collective-permute-start(bf16[1024,256]{1,0:T(8,128)(2,1)} %collective-permute-done.8), channel_id=1, source_target_pairs={{0,1},{1,2},{2,3},{3,4},{4,5},{5,6},{6,7},{7,8},{8,9},{9,10},{10,1... | collective-permute-start | bytes 1572872 | tf_op jit(solution)/shard_map/ppermute | solution.py:64
  81.0 18.3 %collective-permute-start.11 = (bf16[1024,256]{1,0:T(8,128)(2,1)}, bf16[1024,256]{1,0:T(8,128)(2,1)S(1)}, u32[]{:S(2)}, u32[]{:S(2)}) collective-permute-start(bf16[1024,256]{1,0:T(8,128)(2,1)} %collective-permute-done.9), channel_id=1, source_target_pairs={{0,15},{1,0},{2,1},{3,2},{4,3},{5,4},{6,5},{7,6},{8,7},{9,8},{10,9... | collective-permute-start | bytes 1572872 | tf_op jit(solution)/shard_map/ppermute | solution.py:69
  89.6 18.2 %collective-permute-start.12 = (bf16[1024,256]{1,0:T(8,128)(2,1)S(1)}, bf16[1024,256]{1,0:T(8,128)(2,1)S(1)}, u32[]{:S(2)}, u32[]{:S(2)}) collective-permute-start(bf16[1024,256]{1,0:T(8,128)(2,1)S(1)} %collective-permute-done.10), channel_id=1, source_target_pairs={{0,1},{1,2},{2,3},{3,4},{4,5},{5,6},{6,7},{7,8},{8,9},{9,10},{10,1... | collective-permute-start | bytes 1572872 | tf_op jit(solution)/shard_map/ppermute | solution.py:64
  99.3 15.1 %collective-permute-start.13 = (bf16[1024,256]{1,0:T(8,128)(2,1)S(1)}, bf16[1024,256]{1,0:T(8,128)(2,1)S(1)}, u32[]{:S(2)}, u32[]{:S(2)}) collective-permute-start(bf16[1024,256]{1,0:T(8,128)(2,1)S(1)} %collective-permute-done.11), channel_id=1, source_target_pairs={{0,15},{1,0},{2,1},{3,2},{4,3},{5,4},{6,5},{7,6},{8,7},{9,8},{10,9... | collective-permute-start | bytes 1572872 | tf_op jit(solution)/shard_map/ppermute | solution.py:69
  107.9 13.2 %collective-permute-start.14 = (bf16[1024,256]{1,0:T(8,128)(2,1)S(1)}, bf16[1024,256]{1,0:T(8,128)(2,1)S(1)}, u32[]{:S(2)}, u32[]{:S(2)}) collective-permute-start(bf16[1024,256]{1,0:T(8,128)(2,1)S(1)} %collective-permute-done.12), channel_id=1, source_target_pairs={{0,1},{1,2},{2,3},{3,4},{4,5},{5,6},{6,7},{7,8},{8,9},{9,10},{10,1... | collective-permute-start | bytes 1572872 | tf_op jit(solution)/shard_map/ppermute | solution.py:64
  127.9 41.8 %copy-start.4 = (bf16[2,256]{1,0:T(2,128)(2,1)S(1)}, bf16[2,256]{1,0:T(2,128)(2,1)}, u32[]{:S(2)}) copy-start(bf16[2,256]{1,0:T(2,128)(2,1)} %param.14) | copy-start | bytes 3076
  127.9 60.1 %copy-start.6 = (f32[256]{0:T(256)S(1)}, f32[256]{0:T(256)}, u32[]{:S(2)}) copy-start(f32[256]{0:T(256)} %param.15) | copy-start | bytes 3076
  135.2 47.5 %all-to-all-start.1 = ((f32[32,2,2,128]{3,2,1,0:T(2,128)}), f32[32,2,2,128]{3,2,1,0:T(2,128)S(1)}, u32[]{:S(2)}, u32[]{:S(2)}) async-start(f32[32,2,2,128]{3,2,1,0:T(2,128)} %broadcast_in_dim.7), calls=%async_computation.1 | async-start | bytes 131072 | tf_op jit(solution)/shard_map/all_to_all | solution.py:22
  182.6 21.3 %all-to-all-start = ((bf16[32,2,2,4,128]{4,3,2,1,0:T(4,128)(2,1)}), bf16[32,2,2,4,128]{4,3,2,1,0:T(4,128)(2,1)S(1)}, u32[]{:S(2)}, u32[]{:S(2)}) async-start(bf16[32,2,2,4,128]{4,3,2,1,0:T(4,128)(2,1)} %multiply_convert_fusion.2), calls=%async_computation | async-start | bytes 262144 | tf_op jit(solution)/shard_map/all_to_all | solution.py:16
  (2 other events, 16.0 us)
